TPU v7x, 32 devices: a whole 2x2x4 slice. The times are simulated.
32 devices in a mesh: grp: 2 (over y), fs: 4 (over z), tp: 4 (over x, core).
Axes of the slice: x: 2, y: 2, z: 4, core: 2. Of those that a mesh axis runs over, the one named last changes fastest.
Arguments:
- tokens: bfloat16 [3072, 2048], P(('grp', 'fs'), 'tp'), parts along dimension 0, may hold values from -6 to 6
- norm_gain: float32 [2048], P('fs'), may hold values from 0.1 to 1.9
- gate_weight: float32 [32, 2048, 1024], P(None, 'fs', 'tp'), may hold values from -0.125 to 0.125
- up_weight: float32 [32, 2048, 1024], P(None, 'fs', 'tp'), may hold values from -0.125 to 0.125
- down_weight: float32 [32, 1024, 2048], P(None, 'fs', 'tp'), may hold values from -0.1875 to 0.1875
- routes: int32 [3072, 2], P(('grp', 'fs')), parts along dimension 0, may hold values from 0 to 31, as said below
- route_weights: float32 [3072, 2], P(('grp', 'fs')), parts along dimension 0, may hold values from 0.2 to 1
Outputs:
- gate_serve: bfloat16 [64, 2048, 1024], P(('grp', 'fs'), None, 'tp'), parts along dimension 0
- up_serve: bfloat16 [64, 2048, 1024], P(('grp', 'fs'), None, 'tp'), parts along dimension 0
- down_serve: bfloat16 [64, 1024, 2048], P(('grp', 'fs'), None, 'tp'), parts along dimension 0
- mixture: bfloat16 [3072, 2048], P(('grp', 'fs'), 'tp'), parts along dimension 0
There are 2 independent parts, one for each index of `grp`. A program takes and returns all parts, laid end to end along the dimension named above; an argument that names none is the same for every part. Nothing has to cross between parts.
Inputs may be any that keep to these rules, and one draw needn't show every extreme that they name: `routes`: each row names two different experts of one group (expert e lies in group e // 8). In each aligned block of 384 rows no expert is named more than 36 times, and every expert of one group is named exactly 36 times.
All inputs are finite; a program needn't handle non-finite values.
Results may differ from a plain program's by a relative error of at most 0.0087.
Values may be sent and summed in bfloat16 or wider, within the bound.
A program may use at most 192 MiB of HBM per device.

v0:
```python
import jax
import jax.numpy as jnp
from jax import lax
from jax.sharding import PartitionSpec as P

CAP = 36


epsilon = 1e-06


def normalize(rows):
    values = rows.astype(jnp.float32)
    scale = lax.rsqrt(jnp.mean(values * values, axis=-1, keepdims=True) + epsilon)
    return (values * scale).astype(jnp.bfloat16)


def shards(tokens, norm_gain, gate_weight, up_weight, down_weight, routes, route_weights):
    experts = gate_weight.shape[0]
    n_shards = lax.axis_size("fs")
    local_experts = experts // n_shards
    tok_rows = tokens.shape[0]
    gate_low = (norm_gain[None, :, None] * gate_weight).astype(jnp.bfloat16)
    up_low = (norm_gain[None, :, None] * up_weight).astype(jnp.bfloat16)
    down_low = down_weight.astype(jnp.bfloat16)
    gate_serve, up_serve, down_serve = (
        lax.all_to_all(gate_low, "fs", split_axis=0, concat_axis=1, tiled=True),
        lax.all_to_all(up_low, "fs", split_axis=0, concat_axis=1, tiled=True),
        lax.all_to_all(down_low, "fs", split_axis=0, concat_axis=1, tiled=True),
    )
    flat_routes = routes.reshape(-1)
    expert_ids = lax.iota(jnp.int32, experts)
    onehot = (flat_routes[:, None] == expert_ids[None, :]).astype(jnp.int32)
    position = jnp.sum((jnp.cumsum(onehot, axis=0) - 1) * onehot, axis=1)
    slot_index = (flat_routes * CAP + position).reshape(tok_rows, 2)
    slot_ids = lax.iota(jnp.int32, experts * CAP)
    select = jnp.any(slot_ids[:, None, None] == slot_index[None, :, :], axis=2).astype(jnp.bfloat16)
    outbound = jnp.dot(select, tokens, preferred_element_type=jnp.float32).astype(jnp.bfloat16)
    outbound = outbound.reshape(n_shards, local_experts, CAP, outbound.shape[1])
    arrived = lax.all_to_all(outbound, "fs", split_axis=0, concat_axis=2, tiled=True)[0]
    expert_rows = normalize(lax.all_gather(arrived, "tp", axis=2, tiled=True))
    gate_part = jnp.einsum(
        "erd,edh->erh", expert_rows, gate_serve, preferred_element_type=jnp.float32
    )
    up_part = jnp.einsum("erd,edh->erh", expert_rows, up_serve, preferred_element_type=jnp.float32)
    hidden = (jax.nn.silu(gate_part) * up_part).astype(jnp.bfloat16)
    expert_out = jnp.einsum(
        "erk,ekd->erd",
        lax.all_gather(hidden, "tp", axis=2, tiled=True),
        down_serve,
        preferred_element_type=jnp.float32,
    ).astype(jnp.bfloat16)
    expert_out = expert_out.reshape(1, local_experts, hidden.shape[1], expert_out.shape[2])
    returned_rows = lax.all_to_all(expert_out, "fs", split_axis=2, concat_axis=0, tiled=True)
    returned_rows = returned_rows.reshape(experts * CAP, returned_rows.shape[3])
    picked = returned_rows[slot_index]
    mixture = jnp.sum(route_weights[:, :, None] * picked.astype(jnp.float32), axis=1).astype(
        jnp.bfloat16
    )
    return (gate_serve, up_serve, down_serve, mixture)


def solution(mesh):
    in_specs = (
        P(("grp", "fs"), "tp"),
        P("fs"),
        P(None, "fs", "tp"),
        P(None, "fs", "tp"),
        P(None, "fs", "tp"),
        P(("grp", "fs"), None),
        P(("grp", "fs"), None),
    )
    out_specs = (
        P(("grp", "fs"), None, "tp"),
        P(("grp", "fs"), None, "tp"),
        P(("grp", "fs"), None, "tp"),
        P(("grp", "fs"), "tp"),
    )
    return jax.shard_map(shards, mesh=mesh, in_specs=in_specs, out_specs=out_specs, check_vma=False)
```

profile of v0, /device:TPU:0, one launch (start us, length us, event | category | flops | bytes accessed | tf_op | source)
XLA Modules:
  0.0 676.5 jit_solution(1366728823692263623)
XLA Ops:
  8.4 1.7 reduce-window.6
  13.3 1.4 copy.83
  14.7 6.3 all-to-all-start.3
  21.1 17.3 %multiply_convert_fusion = (bf16[32,512,256]{2,1,0:T(8,128)(2,1)}, bf16[32,512,256]{2,1,0:T(8,128)(2,1)}) fusion(f32[32,512,256]{2,1,0:T(8,128)} %param.10, f32[512]{0:T(512)S(1)} %copy-done.5, f32[32,512,256]{2,1,0:T(8,128)} %param.9), kind=kLoop, calls=%fused_computation.1 | loop fusion | flops 16777216 | bytes 50333696 | tf_op jit(solution)/shard_map/convert_element_type | solution.py:24
  38.4 11.2 %all-to-all-done.3 = bf16[4,8,36,512]{3,1,2,0:T(8,128)(2,1)S(1)} async-done(((bf16[4,8,36,512]{3,1,2,0:T(8,128)(2,1)}), bf16[4,8,36,512]{3,1,2,0:T(8,128)(2,1)S(1)}, u32[]{:S(2)}, u32[]{:S(2)}) %all-to-all-start.3) | async-done | bytes 1179680 | tf_op jit(solution)/shard_map/all_to_all | solution.py:40
  49.6 190.1 %all_to_all.84 = bf16[32,512,256]{2,1,0:T(8,128)(2,1)} all-to-all(bf16[32,512,256]{2,1,0:T(8,128)(2,1)} %get-tuple-element.7), channel_id=1, replica_groups=mesh['grp'=2,'fs'=4,'tp'=4] {'fs'}, dimensions={0} | all-to-all | bytes 16777216 | tf_op jit(solution)/shard_map/all_to_all | solution.py:27
  239.7 5.6 all-to-all-start.1
  246.1 9.0 %convert_element_type.38 = bf16[32,256,512]{2,1,0:T(8,128)(2,1)} convert(f32[32,256,512]{2,1,0:T(8,128)} %param.11) | non-fusion elementwise | flops 4194304 | bytes 25165824 | tf_op jit(solution)/shard_map/convert_element_type | solution.py:25
  255.0 172.4 %all-to-all-done.1 = bf16[32,512,256]{2,1,0:T(8,128)(2,1)} async-done(((bf16[32,512,256]{2,1,0:T(8,128)(2,1)}), bf16[32,512,256]{2,1,0:T(8,128)(2,1)}, u32[]{:S(2)}, u32[]{:S(2)}) %all-to-all-start.1) | async-done | bytes 8388640 | tf_op jit(solution)/shard_map/all_to_all | solution.py:28
  427.4 5.6 all-to-all-start.2
  433.3 3.3 fusion
  436.8 3.2 fusion.1
  440.0 7.7 %copy.75 = bf16[4,8,512,256]{3,2,0,1:T(8,128)(2,1)} copy(bf16[4,8,512,256]{3,2,1,0:T(8,128)(2,1)} %bitcast.48) | data formatting | bytes 16777216 | tf_op jit(solution)/shard_map/all_to_all | solution.py:27
  447.7 7.7 %copy.76 = bf16[4,8,512,256]{3,2,0,1:T(8,128)(2,1)} copy(bf16[4,8,512,256]{3,2,1,0:T(8,128)(2,1)} %bitcast.3) | data formatting | bytes 16777216 | tf_op jit(solution)/shard_map/all_to_all | solution.py:28
  455.3 6.8 fusion.4
  462.1 4.1 fusion.11
  466.2 149.5 %all-to-all-done.2 = bf16[32,256,512]{2,1,0:T(8,128)(2,1)} async-done(((bf16[32,256,512]{2,1,0:T(8,128)(2,1)}), bf16[32,256,512]{2,1,0:T(8,128)(2,1)}, u32[]{:S(2)}, u32[]{:S(2)}) %all-to-all-start.2) | async-done | bytes 8388640 | tf_op jit(solution)/shard_map/all_to_all | solution.py:29
  615.7 7.7 %copy.77 = bf16[4,8,256,512]{3,2,0,1:T(8,128)(2,1)} copy(bf16[4,8,256,512]{3,2,1,0:T(8,128)(2,1)} %bitcast.6) | data formatting | bytes 16777216 | tf_op jit(solution)/shard_map/all_to_all | solution.py:29
  623.4 5.5 fusion.7
  628.9 1.7 copy.88
  630.5 3.5 all-to-all-start.4
  634.5 27.6 %all-to-all-done.4 = bf16[1,8,144,512]{3,1,0,2:T(8,128)(2,1)S(1)} async-done(((bf16[1,8,144,512]{3,1,0,2:T(8,128)(2,1)}), bf16[1,8,144,512]{3,1,0,2:T(8,128)(2,1)S(1)}, u32[]{:S(2)}, u32[]{:S(2)}) %all-to-all-start.4) | async-done | bytes 1179680 | tf_op jit(solution)/shard_map/all_to_all | solution.py:54
  662.8 2.7 gather_fusion
  666.5 3.2 multiply_reduce_fusion
  (41 shorter events, 7.6 us)
Async XLA Ops:
  7.2 5.1 copy-start
  12.3 8.8 %copy-start.5 = (f32[512]{0:T(512)S(1)}, f32[512]{0:T(512)}, u32[]{:S(2)}) copy-start(f32[512]{0:T(512)} %param.8) | copy-start | bytes 6148
  14.7 34.9 %all-to-all-start.3 = ((bf16[4,8,36,512]{3,1,2,0:T(8,128)(2,1)}), bf16[4,8,36,512]{3,1,2,0:T(8,128)(2,1)S(1)}, u32[]{:S(2)}, u32[]{:S(2)}) async-start(bf16[4,8,36,512]{3,1,2,0:T(8,128)(2,1)} %copy.83), calls=%async_computation.3 | async-start | bytes 2359296 | tf_op jit(solution)/shard_map/all_to_all | solution.py:40
  49.6 190.1 %copy-start.3 = (bf16[4,8,36,512]{3,1,2,0:T(8,128)(2,1)}, bf16[4,8,36,512]{3,1,2,0:T(8,128)(2,1)S(1)}, u32[]{:S(2)}) copy-start(bf16[4,8,36,512]{3,1,2,0:T(8,128)(2,1)S(1)} %all-to-all-done.3) | copy-start | bytes 3538948
  239.7 187.7 %all-to-all-start.1 = ((bf16[32,512,256]{2,1,0:T(8,128)(2,1)}), bf16[32,512,256]{2,1,0:T(8,128)(2,1)}, u32[]{:S(2)}, u32[]{:S(2)}) async-start(bf16[32,512,256]{2,1,0:T(8,128)(2,1)} %get-tuple-element.6), calls=%async_computation.1 | async-start | bytes 16777216 | tf_op jit(solution)/shard_map/all_to_all | solution.py:28
  245.3 188.0 %all-gather.3.cloned.1.call-start = ((), (), s32[]{:S(2)}) async-start(), calls=%async_computation.5 | async-start | bytes 5898240 | tf_op jit(solution)/shard_map/all_gather | solution.py:41
  427.4 188.3 %all-to-all-start.2 = ((bf16[32,256,512]{2,1,0:T(8,128)(2,1)}), bf16[32,256,512]{2,1,0:T(8,128)(2,1)}, u32[]{:S(2)}, u32[]{:S(2)}) async-start(bf16[32,256,512]{2,1,0:T(8,128)(2,1)} %convert_element_type.38), calls=%async_computation.2 | async-start | bytes 16777216 | tf_op jit(solution)/shard_map/all_to_all | solution.py:29
  433.1 190.3 %all-gather.5.cloned.1.call-start = ((), (), s32[]{:S(2)}) async-start(), calls=%async_computation.6 | async-start | bytes 2949120 | tf_op jit(solution)/shard_map/all_gather | solution.py:49
  455.3 6.8 %copy-start.2 = (bf16[4,8,512,256]{3,2,0,1:T(8,128)(2,1)S(1)}, bf16[4,8,512,256]{3,2,0,1:T(8,128)(2,1)}, u32[]{:S(2)}) copy-start(bf16[4,8,512,256]{3,2,0,1:T(8,128)(2,1)} %copy.76) | copy-start | bytes 25165828
  628.9 5.5 copy-start.4
  630.5 31.6 %all-to-all-start.4 = ((bf16[1,8,144,512]{3,1,0,2:T(8,128)(2,1)}), bf16[1,8,144,512]{3,1,0,2:T(8,128)(2,1)S(1)}, u32[]{:S(2)}, u32[]{:S(2)}) async-start(bf16[1,8,144,512]{3,1,0,2:T(8,128)(2,1)} %copy.88), calls=%async_computation.4 | async-start | bytes 2359296 | tf_op jit(solution)/shard_map/all_to_all | solution.py:54
  662.5 7.2 %copy-start.1 = (bf16[384,512]{1,0:T(8,128)(2,1)S(1)}, bf16[384,512]{1,0:T(8,128)(2,1)}, u32[]{:S(2)}) copy-start(bf16[384,512]{1,0:T(8,128)(2,1)} %param.7) | copy-start | bytes 1179652
Sparse Core Ops, SparseCore 0:
  248.3 38.8 all-gather.2
  466.3 25.4 all-gather.4
where the time goes:
time: 677 us
  waiting for transfers between devices  361 us (53%)
  blocking collectives  190 us (28%)
  other arithmetic  39.4 us (6%)
  local copies, waits for them, and re-layouts  32.9 us (5%)
  starting transfers between devices  21.4 us (3%)
  matrix products  17.1 us (3%)
  between operations  14.3 us (2%)
    all_to_all x1, blocking collectives, shards(): lax.all_to_all(gate_low, 'fs', split_axis=0, concat_axis=1, tiled=True)  190 us
    all_to_all x1, waiting for transfers between devices, shards(): lax.all_to_all(up_low, 'fs', split_axis=0, concat_axis=1, tiled=True)  172 us
    all_to_all x1, waiting for transfers between devices, shards(): lax.all_to_all(down_low, 'fs', split_axis=0, concat_axis=1, tiled=True)  149 us
    all_to_all x1, waiting for transfers between devices, shards(): lax.all_to_all(expert_out, 'fs', split_axis=2, concat_axis=0, tiled=True)  27.6 us
    convert_element_type x1, other arithmetic, shards(): up_low = (norm_gain[None, :, None] * up_weight).astype(jnp.bfloat16)  17.3 us
  transfers between devices with their start and end apart: 6, of which 4 were waited for; matrix products, arithmetic and copies ran while one was open for 10% of the time, Pallas kernels for 0%

commit v1 on v0

--- a/solution.py
+++ b/solution.py
@@ -4,6 +4,7 @@
 from jax.sharding import PartitionSpec as P
 
 CAP = 36
+GROUP = 8
 
 
 epsilon = 1e-06
@@ -15,10 +16,119 @@
     return (values * scale).astype(jnp.bfloat16)
 
 
+def positions(ids, count):
+    onehot = (ids[:, None] == lax.iota(jnp.int32, count)[None, :]).astype(jnp.int32)
+    return jnp.sum((jnp.cumsum(onehot, axis=0) - 1) * onehot, axis=1)
+
+
+def regroup(weight, gain, pieces, last):
+    n_shards = lax.axis_size("fs")
+    me, part = lax.axis_index("fs"), lax.axis_index("grp")
+    experts, rows, cols = weight.shape
+    local = experts // n_shards
+    half = local // 2
+    cuts = [half * i // pieces[-1] for i in pieces]
+    by_dest = weight.reshape(n_shards, local, rows, cols)
+
+    def low(block):
+        if gain is not None:
+            block = gain[:, None] * block
+        return block.astype(jnp.bfloat16)
+
+    own = low(lax.dynamic_index_in_dim(by_dest, me, 0, keepdims=False))
+    out = jnp.broadcast_to(own[:, None], (local, n_shards, rows, cols))
+    for start, end in zip(cuts[:-1], cuts[1:]):
+        first = part * half + start
+        theirs = (1 - part) * half + start
+        send = low(lax.dynamic_slice_in_dim(by_dest, first, end - start, 1))
+        if last is not None:
+            send, last = lax.optimization_barrier((send, last))
+        got = lax.all_to_all(send, "fs", split_axis=0, concat_axis=0, tiled=True)
+        sources = [lax.rem(me + 1 + i, n_shards) for i in range(n_shards - 1)]
+        remote = jnp.stack([lax.dynamic_index_in_dim(got, s, 0, keepdims=False) for s in sources])
+        last = remote
+        swapped = lax.ppermute(remote, "grp", [(0, 1), (1, 0)])
+        out = lax.dynamic_update_slice(out, got.swapaxes(0, 1), (first, 0, 0, 0))
+        for i, s in enumerate(sources):
+            out = lax.dynamic_update_slice(out, swapped[i][:, None], (theirs, s, 0, 0))
+    return out.reshape(local, n_shards * rows, cols), last
+
+
+def grouped(tokens, norm_gain, gate_weight, up_weight, down_weight, routes, route_weights):
+    experts = gate_weight.shape[0]
+    n_shards = lax.axis_size("fs")
+    me = lax.axis_index("fs")
+    local_experts = experts // n_shards
+    tok_rows = tokens.shape[0]
+    room = CAP * local_experts // 2
+    span = n_shards * CAP
+    gate_serve, last = regroup(gate_weight, norm_gain, (0, 1), None)
+
+    flat_routes = routes.reshape(-1)
+    place = positions(flat_routes, experts).reshape(tok_rows, 2)
+    row_slot = (routes % local_experts) * span + me * CAP + place
+    dest = routes[:, 0] // local_experts
+    seat = dest * room + positions(dest, n_shards)
+    seats = lax.iota(jnp.int32, n_shards * room)
+    taken = seats[:, None] == seat[None, :]
+    select = taken.astype(jnp.bfloat16)
+    outbound = jnp.dot(select, tokens, preferred_element_type=jnp.float32).astype(jnp.bfloat16)
+    outbound = outbound.reshape(n_shards, room, outbound.shape[1])
+    facts = jnp.concatenate([(row_slot + 1).astype(jnp.float32), route_weights], axis=1)
+    facts = jnp.sum(jnp.where(taken[None], facts.T[:, None, :], 0.0), axis=2)
+    facts = facts.reshape(4, n_shards, room).swapaxes(0, 1)
+    facts, outbound, last = lax.optimization_barrier((facts, outbound, last))
+    arrived = lax.all_to_all(outbound, "fs", split_axis=0, concat_axis=0, tiled=True)
+    facts = lax.all_to_all(facts, "fs", split_axis=0, concat_axis=0, tiled=True)
+    up_serve, last = regroup(up_weight, norm_gain, (0, 1, 2), (facts, arrived))
+    down_serve, last = regroup(down_weight, None, (0, 2, 3, 4), last)
+    facts = facts.swapaxes(0, 1).reshape(4, n_shards * room)
+    first = facts[0].astype(jnp.int32) - 1
+    second = facts[1].astype(jnp.int32) - 1
+    arrived = arrived.reshape(n_shards * room, arrived.shape[2])
+    normed = normalize(lax.all_gather(arrived, "tp", axis=1, tiled=True))
+    slots = lax.iota(jnp.int32, local_experts * span)
+    use_first = slots[None, :] == first[:, None]
+    use_second = slots[None, :] == second[:, None]
+    spread = (use_first | use_second).astype(jnp.bfloat16)
+    expert_rows = lax.dot_general(
+        spread, normed, (((0,), (0,)), ((), ())), preferred_element_type=jnp.float32
+    ).astype(jnp.bfloat16)
+    expert_rows = expert_rows.reshape(local_experts, span, normed.shape[1])
+    gate_part = jnp.einsum(
+        "erd,edh->erh", expert_rows, gate_serve, preferred_element_type=jnp.float32
+    )
+    up_part = jnp.einsum("erd,edh->erh", expert_rows, up_serve, preferred_element_type=jnp.float32)
+    hidden = (jax.nn.silu(gate_part) * up_part).astype(jnp.bfloat16)
+    expert_out = jnp.einsum(
+        "erk,ekd->erd",
+        lax.all_gather(hidden, "tp", axis=2, tiled=True),
+        down_serve,
+        preferred_element_type=jnp.float32,
+    ).astype(jnp.bfloat16)
+    expert_out = expert_out.reshape(local_experts * span, expert_out.shape[2])
+    picked = [
+        jnp.dot(use.astype(jnp.bfloat16), expert_out, preferred_element_type=jnp.float32)
+        for use in (use_first, use_second)
+    ]
+    mixed = facts[2][:, None] * picked[0] + facts[3][:, None] * picked[1]
+    mixed = mixed.astype(jnp.bfloat16).reshape(n_shards, room, expert_out.shape[1])
+    back = lax.all_to_all(mixed, "fs", split_axis=0, concat_axis=0, tiled=True)
+    back = back.reshape(n_shards * room, back.shape[2])
+    mixture = lax.dot_general(
+        select, back, (((0,), (0,)), ((), ())), preferred_element_type=jnp.float32
+    ).astype(jnp.bfloat16)
+    return (gate_serve, up_serve, down_serve, mixture)
+
+
 def shards(tokens, norm_gain, gate_weight, up_weight, down_weight, routes, route_weights):
     experts = gate_weight.shape[0]
     n_shards = lax.axis_size("fs")
     local_experts = experts // n_shards
+    if local_experts % GROUP == 0 and lax.axis_size("grp") == 2:
+        return grouped(
+            tokens, norm_gain, gate_weight, up_weight, down_weight, routes, route_weights
+        )
     tok_rows = tokens.shape[0]
     gate_low = (norm_gain[None, :, None] * gate_weight).astype(jnp.bfloat16)
     up_low = (norm_gain[None, :, None] * up_weight).astype(jnp.bfloat16)
@@ -29,10 +139,7 @@
         lax.all_to_all(down_low, "fs", split_axis=0, concat_axis=1, tiled=True),
     )
     flat_routes = routes.reshape(-1)
-    expert_ids = lax.iota(jnp.int32, experts)
-    onehot = (flat_routes[:, None] == expert_ids[None, :]).astype(jnp.int32)
-    position = jnp.sum((jnp.cumsum(onehot, axis=0) - 1) * onehot, axis=1)
-    slot_index = (flat_routes * CAP + position).reshape(tok_rows, 2)
+    slot_index = (flat_routes * CAP + positions(flat_routes, experts)).reshape(tok_rows, 2)
     slot_ids = lax.iota(jnp.int32, experts * CAP)
     select = jnp.any(slot_ids[:, None, None] == slot_index[None, :, :], axis=2).astype(jnp.bfloat16)
     outbound = jnp.dot(select, tokens, preferred_element_type=jnp.float32).astype(jnp.bfloat16)

time: 677 us -> 450 us (0.66)
  waiting for transfers between devices: 361 us -> 191 us
  blocking collectives: 190 us -> 72 us
  local copies, waits for them, and re-layouts: 32.9 us -> 73.6 us
  matrix products: 17.1 us -> 31.1 us
  starting transfers between devices: 21.4 us -> 34.7 us
  other arithmetic: 39.4 us -> 31.3 us
    all_to_all x4 -> x6, waiting for transfers between devices: 361 us -> 117 us  [the longest x5 109 us: regroup(): got = lax.all_to_all(send, 'fs', split_axis=0, concat_axis=0, tiled=True)]
    all_to_all x1 -> x3, blocking collectives: 190 us -> 72 us  [the longest x1 49.3 us: regroup(): got = lax.all_to_all(send, 'fs', split_axis=0, concat_axis=0, tiled=True)]
    ppermute x0 -> x6, waiting for transfers between devices: none -> 74.2 us  [regroup(): swapped = lax.ppermute(remote, 'grp', [(0, 1), (1, 0)])]
    dynamic_update_slice x0 -> x23, local copies, waits for them, and re-layouts: none -> 41.9 us  [the longest x17 29.1 us: regroup(): out = lax.dynamic_update_slice(out, swapped[i][:, None], (theirs, s, 0, 0))]
    all_to_all x4 -> x0, local copies, waits for them, and re-layouts: 23.4 us -> none  [the longest x1 7.65 us: shards(): lax.all_to_all(gate_low, 'fs', split_axis=0, concat_axis=1, tiled=True)]
    dot_general x4 -> x8, matrix products: 17.1 us -> 31.1 us  [the longest x1 7.34 us: grouped(): jnp.einsum('erd,edh->erh', expert_rows, up_serve, preferred_element_type=...]
    broadcast_in_dim x1 -> x3, local copies, waits for them, and re-layouts: 0.15 us -> 13 us  [regroup(): out = jnp.broadcast_to(own[:, None], (local, n_shards, rows, cols))]
    convert_element_type x4 -> x6, other arithmetic: 29.5 us -> 18.7 us  [the longest x3 18.7 us: low(): return block.astype(jnp.bfloat16)]
  transfers between devices with their start and end apart: 6 -> 14, of which waited for: 4 -> 9; matrix products, arithmetic and copies ran while one was open for 10% -> 25% of each run, Pallas kernels for 0% -> 0%
where the time goes in v1:
time: 450 us; the launch traced here: 448 us
  waiting for transfers between devices  191 us (42%)
  local copies, waits for them, and re-layouts  73.6 us (16%)
  blocking collectives  72 us (16%)
  starting transfers between devices  34.7 us (8%)
  other arithmetic  31.3 us (7%)
  matrix products  31.1 us (7%)
  between operations  14.3 us (3%)
    all_to_all x5, waiting for transfers between devices, regroup(): got = lax.all_to_all(send, 'fs', split_axis=0, concat_axis=0, tiled=True)  109 us
    ppermute x6, waiting for transfers between devices, regroup(): swapped = lax.ppermute(remote, 'grp', [(0, 1), (1, 0)])  74.2 us
    all_to_all x1, blocking collectives, regroup(): got = lax.all_to_all(send, 'fs', split_axis=0, concat_axis=0, tiled=True)  49.3 us
    dynamic_update_slice x17, local copies, waits for them, and re-layouts, regroup(): out = lax.dynamic_update_slice(out, swapped[i][:, None], (theirs, s, 0, 0))  29.1 us
    all_to_all x5, starting transfers between devices, regroup(): got = lax.all_to_all(send, 'fs', split_axis=0, concat_axis=0, tiled=True)  23.8 us
    convert_element_type x3, other arithmetic, low(): return block.astype(jnp.bfloat16)  18.7 us
    all_to_all x1, blocking collectives, grouped(): back = lax.all_to_all(mixed, 'fs', split_axis=0, concat_axis=0, tiled=True)  14.6 us
    broadcast_in_dim x3, local copies, waits for them, and re-layouts, regroup(): out = jnp.broadcast_to(own[:, None], (local, n_shards, rows, cols))  13 us
  transfers between devices with their start and end apart: 14, of which 9 were waited for; matrix products, arithmetic and copies ran while one was open for 25% of the time, Pallas kernels for 0%

profile of v1, /device:TPU:0, one launch (start us, length us, event | category | flops | bytes accessed | tf_op | source)
XLA Modules:
  0.0 448.2 jit_solution(10182320302504852694)
XLA Ops:
  7.2 6.5 %multiply_convert_fusion = bf16[4,4,512,256]{3,2,1,0:T(8,128)(2,1)} fusion(f32[4,8,512,256]{3,2,1,0:T(8,128)} %bitcast.154, s32[]{:T(128)S(6)} %select_n.119, f32[512]{0:T(512)} %param.8), kind=kLoop, calls=%fused_computation | loop fusion | flops 4194304 | bytes 12584964 | tf_op jit(solution)/shard_map/convert_element_type | solution.py:36
  13.7 6.5 %all-to-all-start = ((bf16[4,4,512,256]{3,2,1,0:T(8,128)(2,1)}), bf16[4,4,512,256]{3,2,1,0:T(8,128)(2,1)}, u32[]{:S(2)}, u32[]{:S(2)}) async-start(bf16[4,4,512,256]{3,2,1,0:T(8,128)(2,1)} %multiply_convert_fusion), calls=%async_computation | async-start | bytes 8388608 | tf_op jit(solution)/shard_map/all_to_all | solution.py:46
  27.0 86.6 %all-to-all-done = bf16[4,4,512,256]{3,2,1,0:T(8,128)(2,1)} async-done(((bf16[4,4,512,256]{3,2,1,0:T(8,128)(2,1)}), bf16[4,4,512,256]{3,2,1,0:T(8,128)(2,1)}, u32[]{:S(2)}, u32[]{:S(2)}) %all-to-all-start) | async-done | bytes 4194336 | tf_op jit(solution)/shard_map/all_to_all | solution.py:46
  117.7 8.1 %all_to_all.45 = f32[4,4,144]{2,1,0:T(4,128)S(1)} all-to-all(f32[4,4,144]{2,1,0:T(4,128)S(1)} %copy.127), channel_id=1, replica_groups=mesh['grp'=2,'fs'=4,'tp'=4] {'fs'}, dimensions={0} | all-to-all | bytes 18432 | tf_op jit(solution)/shard_map/all_to_all | solution.py:82
  129.2 5.8 %multiply_convert_fusion.1 = (bf16[4,2,512,256]{3,2,1,0:T(8,128)(2,1)}, bf16[4,2,512,256]{3,2,1,0:T(8,128)(2,1)S(1)}) fusion(f32[4,8,512,256]{3,2,1,0:T(8,128)} %bitcast.152, s32[]{:T(128)S(6)} %select_n.128, f32[512]{0:T(512)S(1)} %copy-done.8, s32[]{:T(128)S(6)} %select_n.119), kind=kLoop, calls=%fused_computation.13 | loop fusion | flops 4194304 | bytes 12584968 | tf_op jit(solution)/shard_map/convert_element_type | solution.py:36
  135.0 8.3 %all-to-all-done.2 = bf16[4,144,512]{2,1,0:T(8,128)(2,1)S(1)} async-done(((bf16[4,144,512]{2,1,0:T(8,128)(2,1)}), bf16[4,144,512]{2,1,0:T(8,128)(2,1)S(1)}, u32[]{:S(2)}, u32[]{:S(2)}) %all-to-all-start.2) | async-done | bytes 589856 | tf_op jit(solution)/shard_map/all_to_all | solution.py:81
  143.3 49.3 %all_to_all.46 = bf16[4,2,512,256]{3,2,1,0:T(8,128)(2,1)S(1)} all-to-all(bf16[4,2,512,256]{3,2,1,0:T(8,128)(2,1)S(1)} %get-tuple-element.13), channel_id=1, replica_groups=mesh['grp'=2,'fs'=4,'tp'=4] {'fs'}, dimensions={0} | all-to-all | bytes 4194304 | tf_op jit(solution)/shard_map/all_to_all | solution.py:46
  208.4 6.4 %fusion.2 = (bf16[8,512,256]{2,1,0:T(8,128)(2,1)}, bf16[8,512,256]{2,1,0:T(8,128)(2,1)S(1)}) fusion(f32[4,8,512,256]{3,2,1,0:T(8,128)} %bitcast.153, s32[]{:T(128)S(6)} %select_n.118, f32[512]{0:T(512)S(1)} %copy-done.8, f32[4,8,512,256]{3,2,1,0:T(8,128)} %bitcast.155), kind=kLoop, calls=%fused_computation.7 | loop fusion | flops 4194304 | bytes 12584964 | tf_op jit(solution)/shard_map/convert_element_type | solution.py:36
  219.1 4.6 %copy_dynamic-update-slice_fusion = bf16[8,4,512,256]{3,2,1,0:T(8,128)(2,1)} fusion(bf16[8,4,512,256]{3,2,1,0:T(8,128)(2,1)} %broadcast_in_dim.26, s32[]{:T(128)S(6)} %select_n.119, bf16[4,4,512,256]{3,2,1,0:T(8,128)(2,1)} %all-to-all-done), kind=kLoop, calls=%fused_computation.10 | loop fusion | bytes 8388612 | tf_op jit(solution)/shard_map/dynamic_update_slice | solution.py:51
  223.9 22.1 %all-to-all-done.4 = bf16[4,2,512,256]{3,2,1,0:T(8,128)(2,1)S(1)} async-done(((bf16[4,2,512,256]{3,2,1,0:T(8,128)(2,1)}), bf16[4,2,512,256]{3,2,1,0:T(8,128)(2,1)S(1)}, u32[]{:S(2)}, u32[]{:S(2)}) %all-to-all-start.4) | async-done | bytes 2097184 | tf_op jit(solution)/shard_map/all_to_all | solution.py:46
  247.5 4.6 %all-to-all-start.5 = ((bf16[4,2,256,512]{3,2,1,0:T(8,128)(2,1)}), bf16[4,2,256,512]{3,2,1,0:T(8,128)(2,1)}, u32[]{:S(2)}, u32[]{:S(2)}) async-start(bf16[4,2,256,512]{3,2,1,0:T(8,128)(2,1)} %dynamic-slice_convert_fusion), calls=%async_computation.5 | async-start | bytes 4194304 | tf_op jit(solution)/shard_map/all_to_all | solution.py:46
  252.1 15.7 %collective-permute-done = bf16[3,4,512,256]{3,2,1,0:T(8,128)(2,1)} collective-permute-done((bf16[3,4,512,256]{3,2,1,0:T(8,128)(2,1)}, bf16[3,4,512,256]{3,2,1,0:T(8,128)(2,1)}, u32[]{:S(2)}, u32[]{:S(2)}) %collective-permute-start) | collective-permute-done | bytes 3145760 | tf_op jit(solution)/shard_map/ppermute | solution.py:50
  284.3 6.6 %convolution_convert_fusion = bf16[1152,2048]{1,0:T(8,128)(2,1)S(1)} fusion(bf16[576,2048]{1,0:T(8,128)(2,1)} %all-gather.3.cloned.1.call-done, f32[576]{0:T(1024)S(1)} %add_rsqrt_fusion, s32[576]{0:T(1024)S(1)} %sub.54, s32[576]{0:T(1024)S(1)} %sub.52), kind=kOutput, calls=%fused_computation.1 | convolution fusion | flops 2725797888 | bytes 7084800 | tf_op jit(solution)/shard_map/dot_general | solution.py:94
  291.4 7.2 %fusion.53 = f32[8,144,256]{2,1,0:T(8,128)} fusion(bf16[8,144,2048]{2,1,0:T(8,128)(2,1)S(1)} %bitcast.156, bf16[8,2048,256]{2,1,0:T(8,128)(2,1)} %bitcast.8), kind=kOutput, calls=%fused_computation.149 | convolution fusion | flops 1207959552 | bytes 14286848 | tf_op jit(solution)/shard_map/erd,edh->erh/dot_general | solution.py:98
  298.6 13.7 %collective-permute-done.1 = bf16[3,2,512,256]{3,2,1,0:T(8,128)(2,1)} collective-permute-done((bf16[3,2,512,256]{3,2,1,0:T(8,128)(2,1)}, bf16[3,2,512,256]{3,2,1,0:T(8,128)(2,1)}, u32[]{:S(2)}, u32[]{:S(2)}) %collective-permute-start.1) | collective-permute-done | bytes 1572896 | tf_op jit(solution)/shard_map/ppermute | solution.py:50
  316.9 4.7 %all-to-all-start.6 = ((bf16[4,1,256,512]{3,2,1,0:T(8,128)(2,1)}), bf16[4,1,256,512]{3,2,1,0:T(8,128)(2,1)S(1)}, u32[]{:S(2)}, u32[]{:S(2)}) async-start(bf16[4,1,256,512]{3,2,1,0:T(8,128)(2,1)} %get-tuple-element.16), calls=%async_computation.6 | async-start | bytes 2097152 | tf_op jit(solution)/shard_map/all_to_all | solution.py:46
  326.8 15.9 %collective-permute-done.2 = bf16[3,2,512,256]{3,2,1,0:T(8,128)(2,1)} collective-permute-done((bf16[3,2,512,256]{3,2,1,0:T(8,128)(2,1)}, bf16[3,2,512,256]{3,2,1,0:T(8,128)(2,1)}, u32[]{:S(2)}, u32[]{:S(2)}) %collective-permute-start.2) | collective-permute-done | bytes 1572896 | tf_op jit(solution)/shard_map/ppermute | solution.py:50
  350.0 4.4 all-to-all-start.7
  354.4 7.3 %fusion.18 = bf16[8,144,256]{2,1,0:T(8,128)(2,1)} fusion(bf16[8,144,2048]{2,1,0:T(8,128)(2,1)} %bitcast.157, bf16[8,2048,256]{2,1,0:T(8,128)(2,1)} %bitcast.29, f32[8,144,256]{2,1,0:T(8,128)} %fusion.53), kind=kOutput, calls=%fused_computation.41 | convolution fusion | flops 1209729024 | bytes 14876672 | tf_op jit(solution)/shard_map/erd,edh->erh/dot_general | solution.py:101
  372.2 13.6 %collective-permute-done.3 = bf16[3,2,256,512]{3,2,1,0:T(8,128)(2,1)} collective-permute-done((bf16[3,2,256,512]{3,2,1,0:T(8,128)(2,1)}, bf16[3,2,256,512]{3,2,1,0:T(8,128)(2,1)}, u32[]{:S(2)}, u32[]{:S(2)}) %collective-permute-start.3) | collective-permute-done | bytes 1572896 | tf_op jit(solution)/shard_map/ppermute | solution.py:50
  392.5 6.0 %collective-permute-done.4 = bf16[3,1,256,512]{3,2,1,0:T(8,128)(2,1)} collective-permute-done((bf16[3,1,256,512]{3,2,1,0:T(8,128)(2,1)S(1)}, bf16[3,1,256,512]{3,2,1,0:T(8,128)(2,1)}, u32[]{:S(2)}, u32[]{:S(2)}) %collective-permute-start.4) | collective-permute-done | bytes 786464 | tf_op jit(solution)/shard_map/ppermute | solution.py:50
  406.6 9.2 %collective-permute-done.5 = bf16[3,1,256,512]{3,2,1,0:T(8,128)(2,1)S(1)} collective-permute-done((bf16[3,1,256,512]{3,2,1,0:T(8,128)(2,1)S(1)}, bf16[3,1,256,512]{3,2,1,0:T(8,128)(2,1)S(1)}, u32[]{:S(2)}, u32[]{:S(2)}) %collective-permute-start.5) | collective-permute-done | bytes 786464 | tf_op jit(solution)/shard_map/ppermute | solution.py:50
  418.0 5.5 %convolution_convert_fusion.1 = bf16[8,144,512]{2,1,0:T(8,128)(2,1)S(1)} fusion(bf16[8,144,1024]{2,1,0:T(8,128)(2,1)} %all-gather.5.cloned.1.call-done, bf16[8,1024,512]{2,1,0:T(8,128)(2,1)} %bitcast.41), kind=kOutput, calls=%fused_computation.32 | convolution fusion | flops 1208549376 | bytes 11927552 | tf_op jit(solution)/shard_map/erk,ekd->erd/dot_general | solution.py:103
  425.4 14.6 %all_to_all.47 = bf16[4,144,512]{2,1,0:T(8,128)(2,1)S(1)} all-to-all(bf16[4,144,512]{2,1,0:T(8,128)(2,1)S(1)} %bitcast.164), channel_id=1, replica_groups=mesh['grp'=2,'fs'=4,'tp'=4] {'fs'}, dimensions={0} | all-to-all | bytes 1179648 | tf_op jit(solution)/shard_map/all_to_all | solution.py:116
  (113 shorter events, 100.6 us)
Async XLA Ops:
  7.2 18.5 %copy-start = (bf16[384,512]{1,0:T(8,128)(2,1)S(1)}, bf16[384,512]{1,0:T(8,128)(2,1)}, u32[]{:S(2)}) copy-start(bf16[384,512]{1,0:T(8,128)(2,1)} %param.7) | copy-start | bytes 1179652
  13.7 6.5 %copy-start.7 = (s32[384,2]{0,1:T(2,128)S(1)}, s32[384,2]{0,1:T(2,128)}, u32[]{:S(2)}) copy-start(s32[384,2]{0,1:T(2,128)} %param.12) | copy-start | bytes 9220
  13.7 11.1 %copy-start.9 = (f32[384,2]{0,1:T(2,128)S(1)}, f32[384,2]{0,1:T(2,128)}, u32[]{:S(2)}) copy-start(f32[384,2]{0,1:T(2,128)} %param.13) | copy-start | bytes 9220
  13.7 99.9 %all-to-all-start = ((bf16[4,4,512,256]{3,2,1,0:T(8,128)(2,1)}), bf16[4,4,512,256]{3,2,1,0:T(8,128)(2,1)}, u32[]{:S(2)}, u32[]{:S(2)}) async-start(bf16[4,4,512,256]{3,2,1,0:T(8,128)(2,1)} %multiply_convert_fusion), calls=%async_computation | async-start | bytes 8388608 | tf_op jit(solution)/shard_map/all_to_all | solution.py:46
  115.7 13.6 %copy-start.8 = (f32[512]{0:T(512)S(1)}, f32[512]{0:T(512)}, u32[]{:S(2)}) copy-start(f32[512]{0:T(512)} %param.8) | copy-start | bytes 6148
  125.7 17.6 %all-to-all-start.2 = ((bf16[4,144,512]{2,1,0:T(8,128)(2,1)}), bf16[4,144,512]{2,1,0:T(8,128)(2,1)S(1)}, u32[]{:S(2)}, u32[]{:S(2)}) async-start(bf16[4,144,512]{2,1,0:T(8,128)(2,1)} %bitcast.15), calls=%async_computation.2 | async-start | bytes 1179648 | tf_op jit(solution)/shard_map/all_to_all | solution.py:81
  143.3 52.0 %copy-start.6 = (bf16[4,144,512]{2,1,0:T(8,128)(2,1)}, bf16[4,144,512]{2,1,0:T(8,128)(2,1)S(1)}, u32[]{:S(2)}) copy-start(bf16[4,144,512]{2,1,0:T(8,128)(2,1)S(1)} %all-to-all-done.2) | copy-start | bytes 1769476
  192.6 1.3 copy-start.2
  195.3 50.7 %all-to-all-start.4 = ((bf16[4,2,512,256]{3,2,1,0:T(8,128)(2,1)}), bf16[4,2,512,256]{3,2,1,0:T(8,128)(2,1)S(1)}, u32[]{:S(2)}, u32[]{:S(2)}) async-start(bf16[4,2,512,256]{3,2,1,0:T(8,128)(2,1)} %get-tuple-element.14), calls=%async_computation.4 | async-start | bytes 4194304 | tf_op jit(solution)/shard_map/all_to_all | solution.py:46
  198.9 83.1 %all-gather.3.cloned.1.call-start = ((), (), s32[]{:S(2)}) async-start(), calls=%async_computation.9 | async-start | bytes 2949120 | tf_op jit(solution)/shard_map/all_gather | solution.py:89
  199.0 68.9 %collective-permute-start = (bf16[3,4,512,256]{3,2,1,0:T(8,128)(2,1)}, bf16[3,4,512,256]{3,2,1,0:T(8,128)(2,1)}, u32[]{:S(2)}, u32[]{:S(2)}) collective-permute-start(bf16[3,4,512,256]{3,2,1,0:T(8,128)(2,1)} %pad_maximum_fusion), channel_id=1, source_target_pairs={{0,16},{16,0},{1,17},{17,1},{2,18},{18,2},{3,19},{19,3},{4,20},{20... | collective-permute-start | bytes 9437192 | tf_op jit(solution)/shard_map/ppermute | solution.py:50
  247.5 66.6 %all-to-all-start.5 = ((bf16[4,2,256,512]{3,2,1,0:T(8,128)(2,1)}), bf16[4,2,256,512]{3,2,1,0:T(8,128)(2,1)}, u32[]{:S(2)}, u32[]{:S(2)}) async-start(bf16[4,2,256,512]{3,2,1,0:T(8,128)(2,1)} %dynamic-slice_convert_fusion), calls=%async_computation.5 | async-start | bytes 4194304 | tf_op jit(solution)/shard_map/all_to_all | solution.py:46
  252.1 24.1 %copy-start.4 = (bf16[8,512,256]{2,1,0:T(8,128)(2,1)S(1)}, bf16[8,512,256]{2,1,0:T(8,128)(2,1)}, u32[]{:S(2)}) copy-start(bf16[8,512,256]{2,1,0:T(8,128)(2,1)} %get-tuple-element.46) | copy-start | bytes 6291460
  274.7 37.6 %collective-permute-start.1 = (bf16[3,2,512,256]{3,2,1,0:T(8,128)(2,1)}, bf16[3,2,512,256]{3,2,1,0:T(8,128)(2,1)}, u32[]{:S(2)}, u32[]{:S(2)}) collective-permute-start(bf16[3,2,512,256]{3,2,1,0:T(8,128)(2,1)} %pad_maximum_fusion.1), channel_id=1, source_target_pairs={{0,16},{16,0},{1,17},{17,1},{2,18},{18,2},{3,19},{19,3},{4,20},{20... | collective-permute-start | bytes 4718600 | tf_op jit(solution)/shard_map/ppermute | solution.py:50
  276.2 4.3 copy-start.3
  290.8 7.7 %copy-start.5 = (bf16[1152,2048]{1,0:T(8,128)(2,1)}, bf16[1152,2048]{1,0:T(8,128)(2,1)S(1)}, u32[]{:S(2)}) copy-start(bf16[1152,2048]{1,0:T(8,128)(2,1)S(1)} %convolution_convert_fusion) | copy-start | bytes 14155780
  290.8 51.8 %collective-permute-start.2 = (bf16[3,2,512,256]{3,2,1,0:T(8,128)(2,1)}, bf16[3,2,512,256]{3,2,1,0:T(8,128)(2,1)}, u32[]{:S(2)}, u32[]{:S(2)}) collective-permute-start(bf16[3,2,512,256]{3,2,1,0:T(8,128)(2,1)} %pad_maximum_fusion.2), channel_id=1, source_target_pairs={{0,16},{16,0},{1,17},{17,1},{2,18},{18,2},{3,19},{19,3},{4,20},{20... | collective-permute-start | bytes 4718600 | tf_op jit(solution)/shard_map/ppermute | solution.py:50
  316.9 32.9 %all-to-all-start.6 = ((bf16[4,1,256,512]{3,2,1,0:T(8,128)(2,1)}), bf16[4,1,256,512]{3,2,1,0:T(8,128)(2,1)S(1)}, u32[]{:S(2)}, u32[]{:S(2)}) async-start(bf16[4,1,256,512]{3,2,1,0:T(8,128)(2,1)} %get-tuple-element.16), calls=%async_computation.6 | async-start | bytes 2097152 | tf_op jit(solution)/shard_map/all_to_all | solution.py:46
  348.2 37.6 %collective-permute-start.3 = (bf16[3,2,256,512]{3,2,1,0:T(8,128)(2,1)}, bf16[3,2,256,512]{3,2,1,0:T(8,128)(2,1)}, u32[]{:S(2)}, u32[]{:S(2)}) collective-permute-start(bf16[3,2,256,512]{3,2,1,0:T(8,128)(2,1)} %pad_maximum_fusion.3), channel_id=1, source_target_pairs={{0,16},{16,0},{1,17},{17,1},{2,18},{18,2},{3,19},{19,3},{4,20},{20... | collective-permute-start | bytes 4718600 | tf_op jit(solution)/shard_map/ppermute | solution.py:50
  350.0 48.5 %all-to-all-start.7 = ((bf16[4,1,256,512]{3,2,1,0:T(8,128)(2,1)}), bf16[4,1,256,512]{3,2,1,0:T(8,128)(2,1)S(1)}, u32[]{:S(2)}, u32[]{:S(2)}) async-start(bf16[4,1,256,512]{3,2,1,0:T(8,128)(2,1)} %get-tuple-element.17), calls=%async_computation.7 | async-start | bytes 2097152 | tf_op jit(solution)/shard_map/all_to_all | solution.py:46
  354.4 63.6 %all-gather.5.cloned.1.call-start = ((), (), s32[]{:S(2)}) async-start(), calls=%async_computation.10 | async-start | bytes 2949120 | tf_op jit(solution)/shard_map/all_gather | solution.py:105
  371.7 26.8 %collective-permute-start.4 = (bf16[3,1,256,512]{3,2,1,0:T(8,128)(2,1)S(1)}, bf16[3,1,256,512]{3,2,1,0:T(8,128)(2,1)}, u32[]{:S(2)}, u32[]{:S(2)}) collective-permute-start(bf16[3,1,256,512]{3,2,1,0:T(8,128)(2,1)S(1)} %pad_maximum_fusion.4), channel_id=1, source_target_pairs={{0,16},{16,0},{1,17},{17,1},{2,18},{18,2},{3,19},{19,3},{4,20},{20... | collective-permute-start | bytes 2359304 | tf_op jit(solution)/shard_map/ppermute | solution.py:50
  400.3 15.5 %collective-permute-start.5 = (bf16[3,1,256,512]{3,2,1,0:T(8,128)(2,1)S(1)}, bf16[3,1,256,512]{3,2,1,0:T(8,128)(2,1)S(1)}, u32[]{:S(2)}, u32[]{:S(2)}) collective-permute-start(bf16[3,1,256,512]{3,2,1,0:T(8,128)(2,1)S(1)} %pad_maximum_fusion.5), channel_id=1, source_target_pairs={{0,16},{16,0},{1,17},{17,1},{2,18},{18,2},{3,19},{19,3},{4,20},{20... | collective-permute-start | bytes 2359304 | tf_op jit(solution)/shard_map/ppermute | solution.py:50
  423.5 17.9 %copy-start.1 = (bf16[384,512]{1,0:T(8,128)(2,1)S(1)}, bf16[384,512]{1,0:T(8,128)(2,1)}, u32[]{:S(2)}) copy-start(bf16[384,512]{1,0:T(8,128)(2,1)} %param.7) | copy-start | bytes 1179652
Sparse Core Ops, SparseCore 0:
  201.3 25.4 all-gather.2
  361.8 24.8 all-gather.4

commit v2 on v1

--- a/solution.py
+++ b/solution.py
@@ -21,7 +21,26 @@
     return jnp.sum((jnp.cumsum(onehot, axis=0) - 1) * onehot, axis=1)
 
 
-def regroup(weight, gain, pieces, last):
+def shift(block, axis, step):
+    size = lax.axis_size(axis)
+    return lax.ppermute(block, axis, [(i, (i + step) % size) for i in range(size)])
+
+
+def spread_blocks(blocks, axis, sign):
+    return [blocks[0]] + [shift(blocks[i], axis, i * sign) for i in range(1, len(blocks))]
+
+
+def gather_last(block, axis):
+    size, me = lax.axis_size(axis), lax.axis_index(axis)
+    width = block.shape[-1]
+    whole = jnp.zeros(block.shape[:-1] + (size * width,), block.dtype)
+    for i, held in enumerate(spread_blocks([block] * size, axis, 1)):
+        start = lax.rem(me - i + size, size) * width
+        whole = lax.dynamic_update_slice_in_dim(whole, held, start, whole.ndim - 1)
+    return whole
+
+
+def regroup(weight, gain, pieces, last, moves):
     n_shards = lax.axis_size("fs")
     me, part = lax.axis_index("fs"), lax.axis_index("grp")
     experts, rows, cols = weight.shape
@@ -48,6 +67,7 @@
         remote = jnp.stack([lax.dynamic_index_in_dim(got, s, 0, keepdims=False) for s in sources])
         last = remote
         swapped = lax.ppermute(remote, "grp", [(0, 1), (1, 0)])
+        moves.append(first)
         out = lax.dynamic_update_slice(out, got.swapaxes(0, 1), (first, 0, 0, 0))
         for i, s in enumerate(sources):
             out = lax.dynamic_update_slice(out, swapped[i][:, None], (theirs, s, 0, 0))
@@ -62,13 +82,17 @@
     tok_rows = tokens.shape[0]
     room = CAP * local_experts // 2
     span = n_shards * CAP
-    gate_serve, last = regroup(gate_weight, norm_gain, (0, 1), None)
+    moves = []
+    gate_serve, last = regroup(gate_weight, norm_gain, (0, 1, 2), None, moves)
+    up_serve, last = regroup(up_weight, norm_gain, (0, 1, 2), last, moves)
+    down_serve, last = regroup(down_weight, None, (0, 2, 3, 4), last, moves)
 
     flat_routes = routes.reshape(-1)
     place = positions(flat_routes, experts).reshape(tok_rows, 2)
     row_slot = (routes % local_experts) * span + me * CAP + place
     dest = routes[:, 0] // local_experts
-    seat = dest * room + positions(dest, n_shards)
+    ahead = lax.rem(dest - me + n_shards, n_shards)
+    seat = ahead * room + positions(dest, n_shards)
     seats = lax.iota(jnp.int32, n_shards * room)
     taken = seats[:, None] == seat[None, :]
     select = taken.astype(jnp.bfloat16)
@@ -77,16 +101,12 @@
     facts = jnp.concatenate([(row_slot + 1).astype(jnp.float32), route_weights], axis=1)
     facts = jnp.sum(jnp.where(taken[None], facts.T[:, None, :], 0.0), axis=2)
     facts = facts.reshape(4, n_shards, room).swapaxes(0, 1)
-    facts, outbound, last = lax.optimization_barrier((facts, outbound, last))
-    arrived = lax.all_to_all(outbound, "fs", split_axis=0, concat_axis=0, tiled=True)
-    facts = lax.all_to_all(facts, "fs", split_axis=0, concat_axis=0, tiled=True)
-    up_serve, last = regroup(up_weight, norm_gain, (0, 1, 2), (facts, arrived))
-    down_serve, last = regroup(down_weight, None, (0, 2, 3, 4), last)
-    facts = facts.swapaxes(0, 1).reshape(4, n_shards * room)
+    facts = jnp.concatenate(spread_blocks(list(facts), "fs", 1), axis=1)
+    arrived = jnp.concatenate(spread_blocks(list(outbound), "fs", 1), axis=0)
     first = facts[0].astype(jnp.int32) - 1
     second = facts[1].astype(jnp.int32) - 1
-    arrived = arrived.reshape(n_shards * room, arrived.shape[2])
-    normed = normalize(lax.all_gather(arrived, "tp", axis=1, tiled=True))
+    whole_rows = gather_last(arrived, "tp")
+    normed = normalize(whole_rows)
     slots = lax.iota(jnp.int32, local_experts * span)
     use_first = slots[None, :] == first[:, None]
     use_second = slots[None, :] == second[:, None]
@@ -102,7 +122,7 @@
     hidden = (jax.nn.silu(gate_part) * up_part).astype(jnp.bfloat16)
     expert_out = jnp.einsum(
         "erk,ekd->erd",
-        lax.all_gather(hidden, "tp", axis=2, tiled=True),
+        gather_last(hidden, "tp"),
         down_serve,
         preferred_element_type=jnp.float32,
     ).astype(jnp.bfloat16)
@@ -113,8 +133,7 @@
     ]
     mixed = facts[2][:, None] * picked[0] + facts[3][:, None] * picked[1]
     mixed = mixed.astype(jnp.bfloat16).reshape(n_shards, room, expert_out.shape[1])
-    back = lax.all_to_all(mixed, "fs", split_axis=0, concat_axis=0, tiled=True)
-    back = back.reshape(n_shards * room, back.shape[2])
+    back = jnp.concatenate(spread_blocks(list(mixed), "fs", -1), axis=0)
     mixture = lax.dot_general(
         select, back, (((0,), (0,)), ((), ())), preferred_element_type=jnp.float32
     ).astype(jnp.bfloat16)

time: 450 us -> 502 us (1.12); the launches traced: 448 us -> 493 us
  blocking collectives: 72 us -> 0 us
  waiting for transfers between devices: 191 us -> 254 us
  starting transfers between devices: 34.7 us -> 86.4 us
  local copies, waits for them, and re-layouts: 73.6 us -> 89.3 us
  between operations: 14.3 us -> 1.04 us
    all_to_all x3 -> x0, blocking collectives: 72 us -> none  [the longest x1 49.3 us: regroup(): got = lax.all_to_all(send, 'fs', split_axis=0, concat_axis=0, tiled=True)]
    ppermute x0 -> x15, waiting for transfers between devices: none -> 69 us  [shift(): lax.ppermute(block, axis, [(i, (i + step) % size) for i in range(size)])]
    all_to_all x5 -> x7, starting transfers between devices: 23.8 us -> 56.6 us  [regroup(): got = lax.all_to_all(send, 'fs', split_axis=0, concat_axis=0, tiled=True)]
    ppermute x0 -> x15, starting transfers between devices: none -> 22.1 us  [shift(): lax.ppermute(block, axis, [(i, (i + step) % size) for i in range(size)])]
    ppermute x6 -> x7, waiting for transfers between devices: 74.2 us -> 86.3 us  [regroup(): swapped = lax.ppermute(remote, 'grp', [(0, 1), (1, 0)])]
    dynamic_update_slice x0 -> x6, local copies, waits for them, and re-layouts: none -> 10.7 us  [gather_last(): whole = lax.dynamic_update_slice_in_dim(whole, held, start, whole.ndim - 1)]
    all_to_all x5 -> x7, waiting for transfers between devices: 109 us -> 98.4 us  [regroup(): got = lax.all_to_all(send, 'fs', split_axis=0, concat_axis=0, tiled=True)]
    all_to_all x1 -> x0, waiting for transfers between devices: 8.28 us -> none  [grouped(): lax.all_to_all(outbound, 'fs', split_axis=0, concat_axis=0, tiled=True)]
  transfers between devices with their start and end apart: 14 -> 29, of which waited for: 9 -> 15; matrix products, arithmetic and copies ran while one was open for 25% -> 25% of each run, Pallas kernels for 0% -> 0%
where the time goes in v2:
time: 502 us; the launch traced here: 493 us
  waiting for transfers between devices  254 us (51%)
  local copies, waits for them, and re-layouts  89.3 us (18%)
  starting transfers between devices  86.4 us (17%)
  other arithmetic  31.6 us (6%)
  matrix products  30.6 us (6%)
    all_to_all x7, waiting for transfers between devices, regroup(): got = lax.all_to_all(send, 'fs', split_axis=0, concat_axis=0, tiled=True)  98.4 us
    ppermute x7, waiting for transfers between devices, regroup(): swapped = lax.ppermute(remote, 'grp', [(0, 1), (1, 0)])  86.3 us
    ppermute x15, waiting for transfers between devices, shift(): lax.ppermute(block, axis, [(i, (i + step) % size) for i in range(size)])  69 us
    all_to_all x7, starting transfers between devices, regroup(): got = lax.all_to_all(send, 'fs', split_axis=0, concat_axis=0, tiled=True)  56.6 us
    dynamic_update_slice x19, local copies, waits for them, and re-layouts, regroup(): out = lax.dynamic_update_slice(out, swapped[i][:, None], (theirs, s, 0, 0))  24.8 us
    ppermute x15, starting transfers between devices, shift(): lax.ppermute(block, axis, [(i, (i + step) % size) for i in range(size)])  22.1 us
    convert_element_type x2, other arithmetic, low(): return block.astype(jnp.bfloat16)  16.3 us
    dynamic_update_slice x7, local copies, waits for them, and re-layouts, regroup(): out = lax.dynamic_update_slice(out, got.swapaxes(0, 1), (first, 0, 0, 0))  15.5 us
  transfers between devices with their start and end apart: 29, of which 15 were waited for; matrix products, arithmetic and copies ran while one was open for 25% of the time, Pallas kernels for 0%

profile of v2, /device:TPU:0, one launch (start us, length us, event | category | flops | bytes accessed | tf_op | source)
XLA Modules:
  0.0 492.6 jit_solution(1989877392678118250)
XLA Ops:
  0.7 9.8 %multiply_convert_fusion = (bf16[4,2,512,256]{3,2,1,0:T(8,128)(2,1)}, bf16[4,2,512,256]{3,2,1,0:T(8,128)(2,1)}, bf16[4,2,512,256]{3,2,1,0:T(8,128)(2,1)}, bf16[4,2,512,256]{3,2,1,0:T(8,128)(2,1)}) fusion(f32[4,8,512,256]{3,2,1,0:T(8,128)} %bitcast.181, s32[]{:T(128)S(6)} %select_n.158, f32[512]{0:T(512)} %param.8, s32[]{:T(128)S(6)} %select_n.153, ...), kind=kLoop, calls=%fused_computation.11 | loop fusion | flops 8388608 | bytes 25167880 | tf_op jit(solution)/shard_map/convert_element_type | solution.py:55
  10.5 6.3 %all-to-all-start = ((bf16[4,2,512,256]{3,2,1,0:T(8,128)(2,1)}), bf16[4,2,512,256]{3,2,1,0:T(8,128)(2,1)S(1)}, u32[]{:S(2)}, u32[]{:S(2)}) async-start(bf16[4,2,512,256]{3,2,1,0:T(8,128)(2,1)} %get-tuple-element.63), calls=%async_computation | async-start | bytes 4194304 | tf_op jit(solution)/shard_map/all_to_all | solution.py:65
  16.9 48.2 %all-to-all-done = bf16[4,2,512,256]{3,2,1,0:T(8,128)(2,1)S(1)} async-done(((bf16[4,2,512,256]{3,2,1,0:T(8,128)(2,1)}), bf16[4,2,512,256]{3,2,1,0:T(8,128)(2,1)S(1)}, u32[]{:S(2)}, u32[]{:S(2)}) %all-to-all-start) | async-done | bytes 2097184 | tf_op jit(solution)/shard_map/all_to_all | solution.py:65
  66.5 4.6 all-to-all-start.1
  71.1 47.8 %all-to-all-done.1 = bf16[4,2,512,256]{3,2,1,0:T(8,128)(2,1)} async-done(((bf16[4,2,512,256]{3,2,1,0:T(8,128)(2,1)}), bf16[4,2,512,256]{3,2,1,0:T(8,128)(2,1)}, u32[]{:S(2)}, u32[]{:S(2)}) %all-to-all-start.1) | async-done | bytes 2097184 | tf_op jit(solution)/shard_map/all_to_all | solution.py:65
  139.3 6.5 %fusion.2 = (bf16[8,512,256]{2,1,0:T(8,128)(2,1)}, bf16[8,512,256]{2,1,0:T(8,128)(2,1)}) fusion(f32[4,8,512,256]{3,2,1,0:T(8,128)} %bitcast.182, s32[]{:T(128)S(6)} %select_n.152, f32[512]{0:T(512)S(1)} %copy-done.15, f32[4,8,512,256]{3,2,1,0:T(8,128)} %bitcast.184), kind=kLoop, calls=%fused_computation.6 | loop fusion | flops 4194304 | bytes 12584964 | tf_op jit(solution)/shard_map/convert_element_type | solution.py:55
  145.8 22.9 %collective-permute-done.10 = bf16[144,512]{1,0:T(8,128)(2,1)S(1)} collective-permute-done((bf16[144,512]{1,0:T(8,128)(2,1)S(1)}, bf16[144,512]{1,0:T(8,128)(2,1)S(1)}, u32[]{:S(2)}, u32[]{:S(2)}) %collective-permute-start.10) | collective-permute-done | bytes 147488 | tf_op jit(solution)/shard_map/ppermute | solution.py:26
  168.7 15.9 %collective-permute-done.11 = bf16[144,512]{1,0:T(8,128)(2,1)S(1)} collective-permute-done((bf16[144,512]{1,0:T(8,128)(2,1)S(1)}, bf16[144,512]{1,0:T(8,128)(2,1)S(1)}, u32[]{:S(2)}, u32[]{:S(2)}) %collective-permute-start.11) | collective-permute-done | bytes 147488 | tf_op jit(solution)/shard_map/ppermute | solution.py:26
  191.7 4.9 all-to-all-start.3
  209.0 22.2 %collective-permute-done.9 = f32[4,144]{1,0:T(4,128)S(1)} collective-permute-done((f32[4,144]{1,0:T(4,128)S(1)}, f32[4,144]{1,0:T(4,128)S(1)}, u32[]{:S(2)}, u32[]{:S(2)}) %collective-permute-start.9) | collective-permute-done | bytes 2336 | tf_op jit(solution)/shard_map/ppermute | solution.py:26
  240.3 8.1 %convolution_convert_fusion = bf16[1152,2048]{1,0:T(8,128)(2,1)} fusion(bf16[576,2048]{1,0:T(8,128)(2,1)} %constant_dynamic-update-slice_fusion.4, f32[576]{0:T(1024)S(1)} %add_rsqrt_fusion, s32[576]{0:T(1024)S(1)} %get-tuple-element.19, s32[576]{0:T(1024)S(1)} %get-tuple-element.18), kind=kOutput, calls=%fused_computation | convolution fusion | flops 2725797888 | bytes 7084800 | tf_op jit(solution)/shard_map/dot_general | solution.py:114
  263.1 10.2 %collective-permute-done = bf16[3,2,512,256]{3,2,1,0:T(8,128)(2,1)S(1)} collective-permute-done((bf16[3,2,512,256]{3,2,1,0:T(8,128)(2,1)S(1)}, bf16[3,2,512,256]{3,2,1,0:T(8,128)(2,1)S(1)}, u32[]{:S(2)}, u32[]{:S(2)}) %collective-permute-start) | collective-permute-done | bytes 1572896 | tf_op jit(solution)/shard_map/ppermute | solution.py:69
  273.2 33.7 %collective-permute-done.2 = bf16[3,2,512,256]{3,2,1,0:T(8,128)(2,1)S(1)} collective-permute-done((bf16[3,2,512,256]{3,2,1,0:T(8,128)(2,1)S(1)}, bf16[3,2,512,256]{3,2,1,0:T(8,128)(2,1)S(1)}, u32[]{:S(2)}, u32[]{:S(2)}) %collective-permute-start.2) | collective-permute-done | bytes 1572896 | tf_op jit(solution)/shard_map/ppermute | solution.py:69
  312.8 16.2 %all-to-all-start.4 = ((bf16[4,2,256,512]{3,2,1,0:T(8,128)(2,1)}), bf16[4,2,256,512]{3,2,1,0:T(8,128)(2,1)S(1)}, u32[]{:S(2)}, u32[]{:S(2)}) async-start(bf16[4,2,256,512]{3,2,1,0:T(8,128)(2,1)} %dynamic-slice_convert_fusion), calls=%async_computation.4 | async-start | bytes 4194304 | tf_op jit(solution)/shard_map/all_to_all | solution.py:65
  334.0 5.2 %collective-permute-done.1 = bf16[3,2,512,256]{3,2,1,0:T(8,128)(2,1)} collective-permute-done((bf16[3,2,512,256]{3,2,1,0:T(8,128)(2,1)}, bf16[3,2,512,256]{3,2,1,0:T(8,128)(2,1)}, u32[]{:S(2)}, u32[]{:S(2)}) %collective-permute-start.1) | collective-permute-done | bytes 1572896 | tf_op jit(solution)/shard_map/ppermute | solution.py:69
  348.1 5.8 %fusion.64 = f32[8,144,256]{2,1,0:T(8,128)} fusion(bf16[8,144,2048]{2,1,0:T(8,128)(2,1)S(1)} %bitcast.188, bf16[8,2048,256]{2,1,0:T(8,128)(2,1)} %bitcast.16), kind=kOutput, calls=%fused_computation.187 | convolution fusion | flops 1207959552 | bytes 14286848 | tf_op jit(solution)/shard_map/erd,edh->erh/dot_general | solution.py:118
  356.9 22.9 %collective-permute-done.3 = bf16[3,2,512,256]{3,2,1,0:T(8,128)(2,1)S(1)} collective-permute-done((bf16[3,2,512,256]{3,2,1,0:T(8,128)(2,1)S(1)}, bf16[3,2,512,256]{3,2,1,0:T(8,128)(2,1)S(1)}, u32[]{:S(2)}, u32[]{:S(2)}) %collective-permute-start.3) | collective-permute-done | bytes 1572896 | tf_op jit(solution)/shard_map/ppermute | solution.py:69
  383.2 15.0 %all-to-all-start.5 = ((bf16[4,1,256,512]{3,2,1,0:T(8,128)(2,1)}), bf16[4,1,256,512]{3,2,1,0:T(8,128)(2,1)S(1)}, u32[]{:S(2)}, u32[]{:S(2)}) async-start(bf16[4,1,256,512]{3,2,1,0:T(8,128)(2,1)} %get-tuple-element.14), calls=%async_computation.5 | async-start | bytes 2097152 | tf_op jit(solution)/shard_map/all_to_all | solution.py:65
  405.3 7.5 %constant_dynamic-update-slice_fusion.3 = (bf16[8,144,1024]{2,1,0:T(8,128)(2,1)}, bf16[8,144,256]{2,1,0:T(8,128)(2,1)}) fusion(bf16[8,144,1024]{2,1,0:T(8,128)(2,1)} %broadcast_in_dim.36, s32[]{:T(128)S(6)} %select_n.170, bf16[8,144,2048]{2,1,0:T(8,128)(2,1)} %bitcast.185, bf16[8,2048,256]{2,1,0:T(8,128)(2,1)} %bitcast.32, f32[8,144,256]{2,1,0:T(8,128)S(1)} %copy-done.5), kind=kOutput, calls=%fused_computation.107 | convolution fusion | flops 1209729024 | bytes 15466500 | tf_op jit(solution)/shard_map/erd,edh->erh/dot_general | solution.py:121
  423.0 5.1 %all-to-all-start.6 = ((bf16[4,1,256,512]{3,2,1,0:T(8,128)(2,1)}), bf16[4,1,256,512]{3,2,1,0:T(8,128)(2,1)}, u32[]{:S(2)}, u32[]{:S(2)}) async-start(bf16[4,1,256,512]{3,2,1,0:T(8,128)(2,1)} %get-tuple-element.15), calls=%async_computation.6 | async-start | bytes 2097152 | tf_op jit(solution)/shard_map/all_to_all | solution.py:65
  445.9 4.8 collective-permute-done.5
  461.4 9.5 %collective-permute-done.6 = bf16[3,1,256,512]{3,2,1,0:T(8,128)(2,1)S(1)} collective-permute-done((bf16[3,1,256,512]{3,2,1,0:T(8,128)(2,1)S(1)}, bf16[3,1,256,512]{3,2,1,0:T(8,128)(2,1)S(1)}, u32[]{:S(2)}, u32[]{:S(2)}) %collective-permute-start.6) | collective-permute-done | bytes 786464 | tf_op jit(solution)/shard_map/ppermute | solution.py:69
  473.0 5.5 %convolution_convert_fusion.1 = bf16[8,144,512]{2,1,0:T(8,128)(2,1)S(1)} fusion(bf16[8,144,1024]{2,1,0:T(8,128)(2,1)} %constant_dynamic-update-slice_fusion, bf16[8,1024,512]{2,1,0:T(8,128)(2,1)} %bitcast.44), kind=kOutput, calls=%fused_computation.35 | convolution fusion | flops 1208549376 | bytes 11927552 | tf_op jit(solution)/shard_map/erk,ekd->erd/dot_general | solution.py:123
  485.8 5.6 %collective-permute-done.20 = bf16[144,512]{1,0:T(8,128)(2,1)S(1)} collective-permute-done((bf16[144,512]{1,0:T(8,128)(2,1)S(1)}, bf16[144,512]{1,0:T(8,128)(2,1)S(1)}, u32[]{:S(2)}, u32[]{:S(2)}) %collective-permute-start.20) | collective-permute-done | bytes 147488 | tf_op jit(solution)/shard_map/ppermute | solution.py:26
  (181 shorter events, 147.5 us)
Async XLA Ops:
  10.5 54.5 %all-to-all-start = ((bf16[4,2,512,256]{3,2,1,0:T(8,128)(2,1)}), bf16[4,2,512,256]{3,2,1,0:T(8,128)(2,1)S(1)}, u32[]{:S(2)}, u32[]{:S(2)}) async-start(bf16[4,2,512,256]{3,2,1,0:T(8,128)(2,1)} %get-tuple-element.63), calls=%async_computation | async-start | bytes 4194304 | tf_op jit(solution)/shard_map/all_to_all | solution.py:65
  66.5 52.4 %all-to-all-start.1 = ((bf16[4,2,512,256]{3,2,1,0:T(8,128)(2,1)}), bf16[4,2,512,256]{3,2,1,0:T(8,128)(2,1)}, u32[]{:S(2)}, u32[]{:S(2)}) async-start(bf16[4,2,512,256]{3,2,1,0:T(8,128)(2,1)} %get-tuple-element.10), calls=%async_computation.1 | async-start | bytes 4194304 | tf_op jit(solution)/shard_map/all_to_all | solution.py:65
  121.7 67.2 %all-to-all-start.2 = ((bf16[4,2,512,256]{3,2,1,0:T(8,128)(2,1)}), bf16[4,2,512,256]{3,2,1,0:T(8,128)(2,1)}, u32[]{:S(2)}, u32[]{:S(2)}) async-start(bf16[4,2,512,256]{3,2,1,0:T(8,128)(2,1)} %get-tuple-element.11), calls=%async_computation.2 | async-start | bytes 4194304 | tf_op jit(solution)/shard_map/all_to_all | solution.py:65
  128.6 40.1 %collective-permute-start.10 = (bf16[144,512]{1,0:T(8,128)(2,1)S(1)}, bf16[144,512]{1,0:T(8,128)(2,1)S(1)}, u32[]{:S(2)}, u32[]{:S(2)}) collective-permute-start(bf16[144,512]{1,0:T(8,128)(2,1)S(1)} %get-tuple-element.58), channel_id=1, source_target_pairs={{0,4},{4,8},{8,12},{12,0},{1,5},{5,9},{9,13},{13,1},{2,6},{6,10},{... | collective-permute-start | bytes 442376 | tf_op jit(solution)/shard_map/ppermute | solution.py:26
  130.6 54.0 %collective-permute-start.11 = (bf16[144,512]{1,0:T(8,128)(2,1)S(1)}, bf16[144,512]{1,0:T(8,128)(2,1)S(1)}, u32[]{:S(2)}, u32[]{:S(2)}) collective-permute-start(bf16[144,512]{1,0:T(8,128)(2,1)S(1)} %get-tuple-element.57), channel_id=1, source_target_pairs={{0,8},{4,12},{8,0},{12,4},{1,9},{5,13},{9,1},{13,5},{2,10},{6,14},... | collective-permute-start | bytes 442376 | tf_op jit(solution)/shard_map/ppermute | solution.py:26
  132.9 51.7 %collective-permute-start.12 = (bf16[144,512]{1,0:T(8,128)(2,1)S(1)}, bf16[144,512]{1,0:T(8,128)(2,1)S(1)}, u32[]{:S(2)}, u32[]{:S(2)}) collective-permute-start(bf16[144,512]{1,0:T(8,128)(2,1)S(1)} %get-tuple-element.56), channel_id=1, source_target_pairs={{0,12},{4,0},{8,4},{12,8},{1,13},{5,1},{9,5},{13,9},{2,14},{6,2},{... | collective-permute-start | bytes 442376 | tf_op jit(solution)/shard_map/ppermute | solution.py:26
  138.2 67.2 %collective-permute-start.7 = (f32[4,144]{1,0:T(4,128)S(1)}, f32[4,144]{1,0:T(4,128)S(1)}, u32[]{:S(2)}, u32[]{:S(2)}) collective-permute-start(f32[4,144]{1,0:T(4,128)S(1)} %bitcast.200), channel_id=1, source_target_pairs={{0,4},{4,8},{8,12},{12,0},{1,5},{5,9},{9,13},{13,1},{2,6},{6,10},{... | collective-permute-start | bytes 6920 | tf_op jit(solution)/shard_map/ppermute | solution.py:26
  138.8 70.2 %collective-permute-start.8 = (f32[4,144]{1,0:T(4,128)S(1)}, f32[4,144]{1,0:T(4,128)S(1)}, u32[]{:S(2)}, u32[]{:S(2)}) collective-permute-start(f32[4,144]{1,0:T(4,128)S(1)} %bitcast.199), channel_id=1, source_target_pairs={{0,8},{4,12},{8,0},{12,4},{1,9},{5,13},{9,1},{13,5},{2,10},{6,14},... | collective-permute-start | bytes 6920 | tf_op jit(solution)/shard_map/ppermute | solution.py:26
  187.4 43.9 %collective-permute-start.13 = (bf16[576,512]{1,0:T(8,128)(2,1)}, bf16[576,512]{1,0:T(8,128)(2,1)}, u32[]{:S(2)}, u32[]{:S(2)}) collective-permute-start(bf16[576,512]{1,0:T(8,128)(2,1)} %get-tuple-element.53), channel_id=1, source_target_pairs={{0,1},{1,2},{2,3},{3,0},{4,5},{5,6},{6,7},{7,4},{8,9},{9,10},{10,1... | collective-permute-start | bytes 1769480 | tf_op jit(solution)/shard_map/ppermute | solution.py:26
  187.4 45.8 %collective-permute-start.14 = (bf16[576,512]{1,0:T(8,128)(2,1)}, bf16[576,512]{1,0:T(8,128)(2,1)S(1)}, u32[]{:S(2)}, u32[]{:S(2)}) collective-permute-start(bf16[576,512]{1,0:T(8,128)(2,1)} %get-tuple-element.53), channel_id=1, source_target_pairs={{0,2},{1,3},{2,0},{3,1},{4,6},{5,7},{6,4},{7,5},{8,10},{9,11},{10,... | collective-permute-start | bytes 1769480 | tf_op jit(solution)/shard_map/ppermute | solution.py:26
  191.7 118.4 %all-to-all-start.3 = ((bf16[4,2,512,256]{3,2,1,0:T(8,128)(2,1)}), bf16[4,2,512,256]{3,2,1,0:T(8,128)(2,1)}, u32[]{:S(2)}, u32[]{:S(2)}) async-start(bf16[4,2,512,256]{3,2,1,0:T(8,128)(2,1)} %get-tuple-element.12), calls=%async_computation.3 | async-start | bytes 4194304 | tf_op jit(solution)/shard_map/all_to_all | solution.py:65
  200.4 33.7 %collective-permute-start.15 = (bf16[576,512]{1,0:T(8,128)(2,1)}, bf16[576,512]{1,0:T(8,128)(2,1)}, u32[]{:S(2)}, u32[]{:S(2)}) collective-permute-start(bf16[576,512]{1,0:T(8,128)(2,1)} %get-tuple-element.53), channel_id=1, source_target_pairs={{0,3},{1,0},{2,1},{3,2},{4,7},{5,4},{6,5},{7,6},{8,11},{9,8},{10,9... | collective-permute-start | bytes 1769480 | tf_op jit(solution)/shard_map/ppermute | solution.py:26
  205.4 25.8 %collective-permute-start.9 = (f32[4,144]{1,0:T(4,128)S(1)}, f32[4,144]{1,0:T(4,128)S(1)}, u32[]{:S(2)}, u32[]{:S(2)}) collective-permute-start(f32[4,144]{1,0:T(4,128)S(1)} %bitcast.201), channel_id=1, source_target_pairs={{0,12},{4,0},{8,4},{12,8},{1,13},{5,1},{9,5},{13,9},{2,14},{6,2},{... | collective-permute-start | bytes 6920 | tf_op jit(solution)/shard_map/ppermute | solution.py:26
  236.0 37.3 %collective-permute-start = (bf16[3,2,512,256]{3,2,1,0:T(8,128)(2,1)S(1)}, bf16[3,2,512,256]{3,2,1,0:T(8,128)(2,1)S(1)}, u32[]{:S(2)}, u32[]{:S(2)}) collective-permute-start(bf16[3,2,512,256]{3,2,1,0:T(8,128)(2,1)S(1)} %copy-done.6), channel_id=1, source_target_pairs={{0,16},{16,0},{1,17},{17,1},{2,18},{18,2},{3,19},{19,3},{4,20},{20... | collective-permute-start | bytes 4718600 | tf_op jit(solution)/shard_map/ppermute | solution.py:69
  237.5 69.4 %collective-permute-start.2 = (bf16[3,2,512,256]{3,2,1,0:T(8,128)(2,1)S(1)}, bf16[3,2,512,256]{3,2,1,0:T(8,128)(2,1)S(1)}, u32[]{:S(2)}, u32[]{:S(2)}) collective-permute-start(bf16[3,2,512,256]{3,2,1,0:T(8,128)(2,1)S(1)} %copy-done.7), channel_id=1, source_target_pairs={{0,16},{16,0},{1,17},{17,1},{2,18},{18,2},{3,19},{19,3},{4,20},{20... | collective-permute-start | bytes 4718600 | tf_op jit(solution)/shard_map/ppermute | solution.py:69
  254.1 85.1 %collective-permute-start.1 = (bf16[3,2,512,256]{3,2,1,0:T(8,128)(2,1)}, bf16[3,2,512,256]{3,2,1,0:T(8,128)(2,1)}, u32[]{:S(2)}, u32[]{:S(2)}) collective-permute-start(bf16[3,2,512,256]{3,2,1,0:T(8,128)(2,1)} %pad_maximum_fusion.1), channel_id=1, source_target_pairs={{0,16},{16,0},{1,17},{17,1},{2,18},{18,2},{3,19},{19,3},{4,20},{20... | collective-permute-start | bytes 4718600 | tf_op jit(solution)/shard_map/ppermute | solution.py:69
  312.8 69.0 %all-to-all-start.4 = ((bf16[4,2,256,512]{3,2,1,0:T(8,128)(2,1)}), bf16[4,2,256,512]{3,2,1,0:T(8,128)(2,1)S(1)}, u32[]{:S(2)}, u32[]{:S(2)}) async-start(bf16[4,2,256,512]{3,2,1,0:T(8,128)(2,1)} %dynamic-slice_convert_fusion), calls=%async_computation.4 | async-start | bytes 4194304 | tf_op jit(solution)/shard_map/all_to_all | solution.py:65
  344.9 34.9 %collective-permute-start.3 = (bf16[3,2,512,256]{3,2,1,0:T(8,128)(2,1)S(1)}, bf16[3,2,512,256]{3,2,1,0:T(8,128)(2,1)S(1)}, u32[]{:S(2)}, u32[]{:S(2)}) collective-permute-start(bf16[3,2,512,256]{3,2,1,0:T(8,128)(2,1)S(1)} %copy-done.8), channel_id=1, source_target_pairs={{0,16},{16,0},{1,17},{17,1},{2,18},{18,2},{3,19},{19,3},{4,20},{20... | collective-permute-start | bytes 4718600 | tf_op jit(solution)/shard_map/ppermute | solution.py:69
  383.2 38.8 %all-to-all-start.5 = ((bf16[4,1,256,512]{3,2,1,0:T(8,128)(2,1)}), bf16[4,1,256,512]{3,2,1,0:T(8,128)(2,1)S(1)}, u32[]{:S(2)}, u32[]{:S(2)}) async-start(bf16[4,1,256,512]{3,2,1,0:T(8,128)(2,1)} %get-tuple-element.14), calls=%async_computation.5 | async-start | bytes 2097152 | tf_op jit(solution)/shard_map/all_to_all | solution.py:65
  402.1 37.2 %collective-permute-start.4 = (bf16[3,2,256,512]{3,2,1,0:T(8,128)(2,1)}, bf16[3,2,256,512]{3,2,1,0:T(8,128)(2,1)}, u32[]{:S(2)}, u32[]{:S(2)}) collective-permute-start(bf16[3,2,256,512]{3,2,1,0:T(8,128)(2,1)} %pad_maximum_fusion.4), channel_id=1, source_target_pairs={{0,16},{16,0},{1,17},{17,1},{2,18},{18,2},{3,19},{19,3},{4,20},{20... | collective-permute-start | bytes 4718600 | tf_op jit(solution)/shard_map/ppermute | solution.py:69
  412.8 18.2 %collective-permute-start.17 = (bf16[8,144,256]{2,1,0:T(8,128)(2,1)}, bf16[8,144,256]{2,1,0:T(8,128)(2,1)}, u32[]{:S(2)}, u32[]{:S(2)}) collective-permute-start(bf16[8,144,256]{2,1,0:T(8,128)(2,1)} %get-tuple-element.68), channel_id=1, source_target_pairs={{0,2},{1,3},{2,0},{3,1},{4,6},{5,7},{6,4},{7,5},{8,10},{9,11},{10,... | collective-permute-start | bytes 1769480 | tf_op jit(solution)/shard_map/ppermute | solution.py:26
  420.3 35.4 %collective-permute-start.18 = (bf16[8,144,256]{2,1,0:T(8,128)(2,1)}, bf16[8,144,256]{2,1,0:T(8,128)(2,1)}, u32[]{:S(2)}, u32[]{:S(2)}) collective-permute-start(bf16[8,144,256]{2,1,0:T(8,128)(2,1)} %get-tuple-element.68), channel_id=1, source_target_pairs={{0,3},{1,0},{2,1},{3,2},{4,7},{5,4},{6,5},{7,6},{8,11},{9,8},{10,9... | collective-permute-start | bytes 1769480 | tf_op jit(solution)/shard_map/ppermute | solution.py:26
  423.0 30.1 %all-to-all-start.6 = ((bf16[4,1,256,512]{3,2,1,0:T(8,128)(2,1)}), bf16[4,1,256,512]{3,2,1,0:T(8,128)(2,1)}, u32[]{:S(2)}, u32[]{:S(2)}) async-start(bf16[4,1,256,512]{3,2,1,0:T(8,128)(2,1)} %get-tuple-element.15), calls=%async_computation.6 | async-start | bytes 2097152 | tf_op jit(solution)/shard_map/all_to_all | solution.py:65
  455.1 15.7 %collective-permute-start.6 = (bf16[3,1,256,512]{3,2,1,0:T(8,128)(2,1)S(1)}, bf16[3,1,256,512]{3,2,1,0:T(8,128)(2,1)S(1)}, u32[]{:S(2)}, u32[]{:S(2)}) collective-permute-start(bf16[3,1,256,512]{3,2,1,0:T(8,128)(2,1)S(1)} %pad_maximum_fusion.6), channel_id=1, source_target_pairs={{0,16},{16,0},{1,17},{17,1},{2,18},{18,2},{3,19},{19,3},{4,20},{20... | collective-permute-start | bytes 2359304 | tf_op jit(solution)/shard_map/ppermute | solution.py:69
  (28 other events, 437.0 us)
